TPU v7x, 32 devices: a whole 2x2x4 slice. The times are simulated.
32 devices in a mesh: fs: 8 (over z, core), tp: 4 (over y, x).
Axes of the slice: x: 2, y: 2, z: 4, core: 2. Of those that a mesh axis runs over, the one named last changes fastest.
Arguments:
- tokens: bfloat16 [1024, 2048], P('fs'), may hold values from -6 to 6
- experts: int32 [1024, 4], P('fs'), may hold values from 0 to 7, all different within a row; in each aligned block of 128 rows (0 to 127, 128 to 255, ...) at most 96 rows name the same one
- routing: float32 [1024, 4], P('fs'), may hold values from 0.05 to 0.6
- norm_gain: float32 [2048], replicated, may hold values from 0.1 to 1.9
- gate_master: float32 [8, 2048, 2048], P(None, 'fs', 'tp'), may hold values from -0.625 to 0.625
- linear_master: float32 [8, 2048, 2048], P(None, 'fs', 'tp'), may hold values from -0.625 to 0.625
- down_weight: bfloat16 [8, 2048, 2048], P('fs', None, 'tp'), may hold values from -0.013671875 to 0.013671875
Outputs:
- gate_out: bfloat16 [8, 2048, 2048], P('fs', None, 'tp')
- linear_out: bfloat16 [8, 2048, 2048], P('fs', None, 'tp')
- expert_mix: bfloat16 [1024, 2048], P('fs', 'tp')
Inputs may be any that keep to these rules, and one draw needn't show every extreme that they name: Each row names 4 different experts; within the rows of one index of fs (aligned blocks of 128 rows) no expert is named by more than 96 rows, and in some blocks some expert is named by exactly 96; every expert is named somewhere.
All inputs are finite; a program needn't handle non-finite values.
Results may differ from a plain program's by a relative error of at most 0.023.
Values may be sent and summed in bfloat16 or wider, within the bound.
A program may use at most 64 MiB of HBM per device.

v0:
```python
import jax
import jax.numpy as jnp
from jax import lax
from jax.sharding import PartitionSpec as P

clamp_limit = 7.0
gate_slope = 1.702


def solution(mesh):
    n_fs, n_tp = (mesh.shape["fs"], mesh.shape["tp"])

    def on_device(tokens, experts, routing, norm_gain, gate_master, linear_master, down_weight):
        expert_count, depth, _ = gate_master.shape
        width = tokens.shape[1]
        fs, tp = (lax.axis_index("fs"), lax.axis_index("tp"))
        cols = width // n_tp
        mine = lax.dynamic_slice_in_dim(tokens, tp * cols, cols, axis=1)
        quarter = lax.all_gather(mine, "fs", axis=0, tiled=True)
        everyone = lax.all_gather(quarter, "tp", axis=1, tiled=True)
        choice = experts[:, :, None] == jnp.arange(expert_count, dtype=jnp.int32)[None, None, :]
        share = jnp.sum(jnp.where(choice, routing[:, :, None], 0.0), axis=1)
        shares = lax.all_gather(share, "fs", axis=0, tiled=True)
        share_mine = lax.dynamic_slice_in_dim(shares, fs, 1, axis=1)
        gain = lax.dynamic_slice_in_dim(norm_gain, fs * depth, depth, axis=0)[None, :, None]
        gate_out, linear_out = (
            lax.all_to_all(
                (master * gain).astype(jnp.bfloat16), "fs", split_axis=0, concat_axis=1, tiled=True
            )
            for master in (gate_master, linear_master)
        )
        pre_gate = jnp.dot(everyone, gate_out[0], preferred_element_type=jnp.float32)
        pre_linear = jnp.dot(everyone, linear_out[0], preferred_element_type=jnp.float32)
        clamped = jnp.minimum(pre_gate, clamp_limit)
        active = (
            clamped
            * jax.nn.sigmoid(gate_slope * clamped)
            * (jnp.clip(pre_linear, -clamp_limit, clamp_limit) + 1.0)
        ).astype(jnp.bfloat16)
        part = lax.dot_general(
            active, down_weight[0], (((1,), (1,)), ((), ())), preferred_element_type=jnp.float32
        )
        part = (part * share_mine).astype(jnp.bfloat16)
        summed = lax.psum_scatter(part, "tp", scatter_dimension=1, tiled=True)
        mixed = lax.psum_scatter(summed, "fs", scatter_dimension=0, tiled=True)
        return (gate_out, linear_out, mixed)

    placed = (
        P("fs", None),
        P("fs", None),
        P("fs", None),
        P(),
        P(None, "fs", "tp"),
        P(None, "fs", "tp"),
        P("fs", None, "tp"),
    )
    return jax.shard_map(
        on_device,
        mesh=mesh,
        in_specs=placed,
        out_specs=(P("fs", None, "tp"), P("fs", None, "tp"), P("fs", "tp")),
        check_vma=False,
    )
```

profile of v0, /device:TPU:0, one launch (start us, length us, event | category | flops | bytes accessed | tf_op | source)
XLA Modules:
  0.0 255.2 jit_solution(7410514343636466735)
XLA Ops:
  7.2 0.0 copy-start
  7.2 0.0 all-gather.3.cloned.1.call-start
  7.2 1.7 constant_dynamic-slice_fusion.1
  8.9 0.0 all-gather.3.cloned.1.call-update
  9.0 0.8 dynamic_slice.9
  9.7 6.8 %multiply_convert_fusion.1 = (bf16[8,256,512]{2,1,0:T(8,128)(2,1)}, bf16[8,256,512]{2,1,0:T(8,128)(2,1)}) fusion(f32[8,256,512]{2,1,0:T(8,128)} %param.12, f32[256]{0:T(256)S(1)} %dynamic_slice.9, f32[8,256,512]{2,1,0:T(8,128)} %param.11), kind=kLoop, calls=%fused_computation.1 | loop fusion | flops 4194304 | bytes 12583936 | tf_op jit(solution)/shard_map/convert_element_type | solution.py:28
  16.5 6.4 %all-to-all-start.1 = ((bf16[8,256,512]{2,1,0:T(8,128)(2,1)}), bf16[8,256,512]{2,1,0:T(8,128)(2,1)}, u32[]{:S(2)}, u32[]{:S(2)}) async-start(bf16[8,256,512]{2,1,0:T(8,128)(2,1)} %get-tuple-element.3), calls=%async_computation.1 | async-start | bytes 4194304 | tf_op jit(solution)/shard_map/all_to_all | solution.py:27
  22.9 0.0 all-gather.5.cloned.1.call-start
  22.9 17.5 %all-gather.3.cloned.1.call-done = bf16[1024,512]{1,0:T(8,128)(2,1)} async-done(((bf16[128,512]{1,0:T(8,128)(2,1)}), bf16[1024,512]{1,0:T(8,128)(2,1)}) %all-gather.3.cloned.1.call-update) | async-done | bytes 1048592 | tf_op jit(solution)/shard_map/all_gather | solution.py:19
  40.4 0.0 all-gather.5.cloned.1.call-update
  40.4 37.4 %all-to-all-done.1 = bf16[8,256,512]{2,1,0:T(8,128)(2,1)} async-done(((bf16[8,256,512]{2,1,0:T(8,128)(2,1)}), bf16[8,256,512]{2,1,0:T(8,128)(2,1)}, u32[]{:S(2)}, u32[]{:S(2)}) %all-to-all-start.1) | async-done | bytes 2097184 | tf_op jit(solution)/shard_map/all_to_all | solution.py:27
  77.8 4.5 %all-to-all-start = ((bf16[8,256,512]{2,1,0:T(8,128)(2,1)}), bf16[8,256,512]{2,1,0:T(8,128)(2,1)}, u32[]{:S(2)}, u32[]{:S(2)}) async-start(bf16[8,256,512]{2,1,0:T(8,128)(2,1)} %get-tuple-element.4), calls=%async_computation | async-start | bytes 4194304 | tf_op jit(solution)/shard_map/all_to_all | solution.py:27
  82.3 0.0 reduce-scatter.3.cloned.1.call-start
  82.4 55.0 %all_gather.11 = f32[1024,8]{0,1:T(8,128)S(1)} all-gather(f32[128,8]{0,1:T(8,128)S(1)} %select_reduce_fusion), channel_id=1, replica_groups=mesh['fs'=8,'tp'=4] {'fs'}, dimensions={0}, use_global_device_ids=true | all-gather | bytes 36864 | tf_op jit(solution)/shard_map/all_gather | solution.py:23
  137.4 0.0 all-gather.5.cloned.1.call-done
  137.5 6.5 %fusion.5 = f32[1024,512]{1,0:T(8,128)} fusion(bf16[1024,2048]{1,0:T(8,128)(2,1)} %all-gather.5.cloned.1.call-done, bf16[2048,512]{1,0:T(8,128)(2,1)} %bitcast.3), kind=kOutput, calls=%fused_computation.13 | convolution fusion | flops 2147483648 | bytes 8388608 | tf_op jit(solution)/shard_map/dot_general | solution.py:33
  144.0 10.3 %multiply_convert_fusion = bf16[1024,2048]{1,0:T(8,128)(2,1)} fusion(f32[1024]{0:T(1024)S(1)} %bitcast.12, bf16[1,2048,512]{2,1,0:T(8,128)(2,1)S(1)} %copy-done, f32[1024,512]{1,0:T(8,128)} %fusion.5, bf16[1024,2048]{1,0:T(8,128)(2,1)} %all-gather.5.cloned.1.call-done, bf16[2048,512]{1,0:T(8,128)(2,1)} %bitcast.2), kind=kOutput, calls=%fused_computation | convolution fusion | flops 4304404480 | bytes 14684160 | tf_op jit(solution)/shard_map/dot_general | solution.py:40
  154.3 0.0 reduce-scatter.3.cloned.1.call-update
  154.3 0.0 reduce-scatter.5.cloned.1.call-start
  154.4 52.8 %reduce-scatter.3.cloned.1.call-done = bf16[1024,512]{1,0:T(8,128)(2,1)} async-done(((bf16[1024,2048]{1,0:T(8,128)(2,1)}), bf16[1024,512]{1,0:T(8,128)(2,1)}) %reduce-scatter.3.cloned.1.call-update) | async-done | bytes 1048592 | tf_op jit(solution)/shard_map/reduce_scatter | solution.py:44
  207.2 0.0 reduce-scatter.5.cloned.1.call-update
  207.2 35.4 %reduce-scatter.5.cloned.1.call-done = bf16[128,512]{1,0:T(8,128)(2,1)} async-done(((bf16[1024,512]{1,0:T(8,128)(2,1)}), bf16[128,512]{1,0:T(8,128)(2,1)}) %reduce-scatter.5.cloned.1.call-update) | async-done | bytes 131088 | tf_op jit(solution)/shard_map/reduce_scatter | solution.py:45
  242.6 3.0 %copy.16 = bf16[1,2048,512]{2,1,0:T(8,128)(2,1)} copy(bf16[1,2048,512]{2,1,0:T(8,128)(2,1)} %bitcast) | data formatting | bytes 4194304
  245.6 3.0 %copy.17 = bf16[1,2048,512]{2,1,0:T(8,128)(2,1)} copy(bf16[1,2048,512]{2,1,0:T(8,128)(2,1)} %bitcast.1) | data formatting | bytes 4194304
  (8 shorter events, 0.0 us)
Async XLA Ops:
  7.2 136.8 %copy-start = (bf16[1,2048,512]{2,1,0:T(8,128)(2,1)S(1)}, bf16[1,2048,512]{2,1,0:T(8,128)(2,1)}, u32[]{:S(2)}) copy-start(bf16[1,2048,512]{2,1,0:T(8,128)(2,1)} %param.13) | copy-start | bytes 6291460
  7.2 33.2 %all-gather.3.cloned.1.call-start = ((), (), s32[]{:S(2)}) async-start(), calls=%async_computation.4 | async-start | bytes 1179648 | tf_op jit(solution)/shard_map/all_gather | solution.py:19
  16.5 61.3 %all-to-all-start.1 = ((bf16[8,256,512]{2,1,0:T(8,128)(2,1)}), bf16[8,256,512]{2,1,0:T(8,128)(2,1)}, u32[]{:S(2)}, u32[]{:S(2)}) async-start(bf16[8,256,512]{2,1,0:T(8,128)(2,1)} %get-tuple-element.3), calls=%async_computation.1 | async-start | bytes 4194304 | tf_op jit(solution)/shard_map/all_to_all | solution.py:27
  22.9 114.6 %all-gather.5.cloned.1.call-start = ((), (), s32[]{:S(2)}) async-start(), calls=%async_computation.5 | async-start | bytes 5242880 | tf_op jit(solution)/shard_map/all_gather | solution.py:20
  77.8 4.6 %copy-start.1 = (f32[128,4]{0,1:T(4,128)S(1)}, f32[128,4]{0,1:T(4,128)}, u32[]{:S(2)}) copy-start(f32[128,4]{0,1:T(4,128)} %param.9) | copy-start | bytes 6148
  77.8 4.6 %copy-start.2 = (s32[128,4]{0,1:T(4,128)S(1)}, s32[128,4]{0,1:T(4,128)}, u32[]{:S(2)}) copy-start(s32[128,4]{0,1:T(4,128)} %param.8) | copy-start | bytes 6148
  77.8 66.2 %all-to-all-start = ((bf16[8,256,512]{2,1,0:T(8,128)(2,1)}), bf16[8,256,512]{2,1,0:T(8,128)(2,1)}, u32[]{:S(2)}, u32[]{:S(2)}) async-start(bf16[8,256,512]{2,1,0:T(8,128)(2,1)} %get-tuple-element.4), calls=%async_computation | async-start | bytes 4194304 | tf_op jit(solution)/shard_map/all_to_all | solution.py:27
  82.3 124.9 %reduce-scatter.3.cloned.1.call-start = ((), (), s32[]{:S(2)}) async-start(), calls=%async_computation.6 | async-start | bytes 5242880 | tf_op jit(solution)/shard_map/reduce_scatter | solution.py:44
  154.3 88.3 %reduce-scatter.5.cloned.1.call-start = ((), (), s32[]{:S(2)}) async-start(), calls=%async_computation.7 | async-start | bytes 1179648 | tf_op jit(solution)/shard_map/reduce_scatter | solution.py:45
Sparse Core Ops, SparseCore 0:
  10.2 30.2 all-gather.2
  42.2 56.2 all-gather.4
  154.4 52.7 reduce-scatter.2
  209.9 32.6 reduce-scatter.4
where the time goes:
time: 256 us; the launch traced here: 255 us
  waiting for transfers between devices  143 us (56%)
  blocking collectives  55 us (21%)
  matrix products  16.8 us (7%)
  between operations  13.8 us (5%)
  starting transfers between devices  11 us (4%)
  local copies, waits for them, and re-layouts  8.59 us (3%)
  other arithmetic  6.81 us (3%)
    all_gather x1, blocking collectives, on_device(): shares = lax.all_gather(share, 'fs', axis=0, tiled=True)  55 us
    reduce_scatter x1, waiting for transfers between devices, on_device(): summed = lax.psum_scatter(part, 'tp', scatter_dimension=1, tiled=True)  52.8 us
    all_to_all x2, waiting for transfers between devices, on_device(): lax.all_to_all((master * gain).astype(jnp.bfloat16), 'fs', split_axis=0,...  37.4 us
    reduce_scatter x1, waiting for transfers between devices, on_device(): mixed = lax.psum_scatter(summed, 'fs', scatter_dimension=0, tiled=True)  35.4 us
    all_gather x1, waiting for transfers between devices, on_device(): quarter = lax.all_gather(mine, 'fs', axis=0, tiled=True)  17.5 us
    all_to_all x2, starting transfers between devices, on_device(): lax.all_to_all((master * gain).astype(jnp.bfloat16), 'fs', split_axis=0,...  10.8 us
    dot_general x1, matrix products, on_device(): lax.dot_general(active, down_weight[0], (((1,), (1,)), ((), ())), preferr...  10.3 us
    convert_element_type x1, other arithmetic, on_device(): (master * gain).astype(jnp.bfloat16)  6.8 us
  transfers between devices with their start and end apart: 6, of which 4 were waited for; matrix products, arithmetic and copies ran while one was open for 6% of the time, Pallas kernels for 0%

commit v1 on v0

--- a/solution.py
+++ b/solution.py
@@ -17,7 +17,9 @@
         cols = width // n_tp
         mine = lax.dynamic_slice_in_dim(tokens, tp * cols, cols, axis=1)
         quarter = lax.all_gather(mine, "fs", axis=0, tiled=True)
-        everyone = lax.all_gather(quarter, "tp", axis=1, tiled=True)
+        everyone = jnp.concatenate(
+            lax.all_to_all(jnp.stack([quarter] * lax.axis_size("tp")), "tp", 0, 0), axis=1
+        )
         choice = experts[:, :, None] == jnp.arange(expert_count, dtype=jnp.int32)[None, None, :]
         share = jnp.sum(jnp.where(choice, routing[:, :, None], 0.0), axis=1)
         shares = lax.all_gather(share, "fs", axis=0, tiled=True)

time: 256 us -> 307 us (1.20)
  blocking collectives: 55 us -> 106 us
    all_to_all x0 -> x1, blocking collectives: none -> 51.2 us  [on_device(): lax.all_to_all(jnp.stack([quarter] * lax.axis_size('tp')), 'tp', 0, 0)]
    all_to_all x2, waiting for transfers between devices: 37.4 us -> 22.1 us  [on_device(): lax.all_to_all((master * gain).astype(jnp.bfloat16), 'fs', split_axis=0,...]
    all_gather x1, waiting for transfers between devices: 17.5 us -> 32.3 us  [on_device(): quarter = lax.all_gather(mine, 'fs', axis=0, tiled=True)]
  transfers between devices with their start and end apart: 6 -> 5, of which waited for: 4 -> 4; matrix products, arithmetic and copies ran while one was open for 6% -> 3% of each run, Pallas kernels for 0% -> 0%
where the time goes in v1:
time: 307 us
  waiting for transfers between devices  141 us (46%)
  blocking collectives  106 us (35%)
  matrix products  16.9 us (6%)
  between operations  13.8 us (4%)
  starting transfers between devices  11 us (4%)
  local copies, waits for them, and re-layouts  10.6 us (3%)
  other arithmetic  6.81 us (2%)
    all_gather x1, blocking collectives, on_device(): shares = lax.all_gather(share, 'fs', axis=0, tiled=True)  55 us
    reduce_scatter x1, waiting for transfers between devices, on_device(): summed = lax.psum_scatter(part, 'tp', scatter_dimension=1, tiled=True)  51.4 us
    all_to_all x1, blocking collectives, on_device(): lax.all_to_all(jnp.stack([quarter] * lax.axis_size('tp')), 'tp', 0, 0)  51.2 us
    reduce_scatter x1, waiting for transfers between devices, on_device(): mixed = lax.psum_scatter(summed, 'fs', scatter_dimension=0, tiled=True)  35.4 us
    all_gather x1, waiting for transfers between devices, on_device(): quarter = lax.all_gather(mine, 'fs', axis=0, tiled=True)  32.3 us
    all_to_all x2, waiting for transfers between devices, on_device(): lax.all_to_all((master * gain).astype(jnp.bfloat16), 'fs', split_axis=0,...  22.1 us
    all_to_all x2, starting transfers between devices, on_device(): lax.all_to_all((master * gain).astype(jnp.bfloat16), 'fs', split_axis=0,...  10.8 us
    dot_general x1, matrix products, on_device(): lax.dot_general(active, down_weight[0], (((1,), (1,)), ((), ())), preferr...  10.3 us
  transfers between devices with their start and end apart: 5, of which 4 were waited for; matrix products, arithmetic and copies ran while one was open for 3% of the time, Pallas kernels for 0%

profile of v1, /device:TPU:0, one launch (start us, length us, event | category | flops | bytes accessed | tf_op | source)
XLA Modules:
  0.0 306.6 jit_solution(14991201083637401240)
XLA Ops:
  7.2 0.0 copy-start
  7.2 0.9 dynamic_slice.9
  8.1 6.8 %multiply_convert_fusion.1 = (bf16[8,256,512]{2,1,0:T(8,128)(2,1)}, bf16[8,256,512]{2,1,0:T(8,128)(2,1)}) fusion(f32[8,256,512]{2,1,0:T(8,128)} %param.12, f32[256]{0:T(256)S(1)} %dynamic_slice.9, f32[8,256,512]{2,1,0:T(8,128)} %param.11), kind=kLoop, calls=%fused_computation.1 | loop fusion | flops 4194304 | bytes 12583936 | tf_op jit(solution)/shard_map/convert_element_type | solution.py:30
  14.9 6.4 %all-to-all-start.1 = ((bf16[8,256,512]{2,1,0:T(8,128)(2,1)}), bf16[8,256,512]{2,1,0:T(8,128)(2,1)}, u32[]{:S(2)}, u32[]{:S(2)}) async-start(bf16[8,256,512]{2,1,0:T(8,128)(2,1)} %get-tuple-element.3), calls=%async_computation.1 | async-start | bytes 4194304 | tf_op jit(solution)/shard_map/all_to_all | solution.py:29
  21.3 0.0 all-gather.2.cloned.1.call-start
  21.3 1.6 constant_dynamic-slice_fusion.1
  22.9 0.0 all-gather.2.cloned.1.call-update
  22.9 32.3 %all-gather.2.cloned.1.call-done = bf16[1024,512]{1,0:T(8,128)(2,1)} async-done(((bf16[128,512]{1,0:T(8,128)(2,1)}), bf16[1024,512]{1,0:T(8,128)(2,1)}) %all-gather.2.cloned.1.call-update) | async-done | bytes 1048592 | tf_op jit(solution)/shard_map/all_gather | solution.py:19
  55.2 1.5 copy.15
  56.7 22.1 %all-to-all-done.1 = bf16[8,256,512]{2,1,0:T(8,128)(2,1)} async-done(((bf16[8,256,512]{2,1,0:T(8,128)(2,1)}), bf16[8,256,512]{2,1,0:T(8,128)(2,1)}, u32[]{:S(2)}, u32[]{:S(2)}) %all-to-all-start.1) | async-done | bytes 2097184 | tf_op jit(solution)/shard_map/all_to_all | solution.py:29
  78.8 0.5 stack.2
  79.3 51.2 %all_to_all.29 = bf16[4,1024,512]{1,2,0:T(8,128)(2,1)} all-to-all(bf16[4,1024,512]{1,2,0:T(8,128)(2,1)S(1)} %stack.2), channel_id=1, replica_groups=mesh['fs'=8,'tp'=4] {'tp'}, dimensions={0} | all-to-all | bytes 8388608 | tf_op jit(solution)/shard_map/all_to_all | solution.py:21
  130.6 4.5 %all-to-all-start = ((bf16[8,256,512]{2,1,0:T(8,128)(2,1)}), bf16[8,256,512]{2,1,0:T(8,128)(2,1)}, u32[]{:S(2)}, u32[]{:S(2)}) async-start(bf16[8,256,512]{2,1,0:T(8,128)(2,1)} %get-tuple-element.4), calls=%async_computation | async-start | bytes 4194304 | tf_op jit(solution)/shard_map/all_to_all | solution.py:29
  135.1 0.0 reduce-scatter.3.cloned.1.call-start
  135.2 55.0 %all_gather.7 = f32[1024,8]{0,1:T(8,128)S(1)} all-gather(f32[128,8]{0,1:T(8,128)S(1)} %select_reduce_fusion), channel_id=1, replica_groups=mesh['fs'=8,'tp'=4] {'fs'}, dimensions={0}, use_global_device_ids=true | all-gather | bytes 36864 | tf_op jit(solution)/shard_map/all_gather | solution.py:25
  190.2 6.6 %fusion.5 = f32[1024,512]{1,0:T(8,128)} fusion(bf16[1024,2048]{0,1:T(8,128)(2,1)} %bitcast.15, bf16[2048,512]{1,0:T(8,128)(2,1)} %bitcast.6), kind=kOutput, calls=%fused_computation.13 | convolution fusion | flops 2147483648 | bytes 8388608 | tf_op jit(solution)/shard_map/dot_general | solution.py:35
  196.8 10.3 %multiply_convert_fusion = bf16[1024,2048]{1,0:T(8,128)(2,1)} fusion(f32[1024]{0:T(1024)S(1)} %bitcast.17, bf16[1,2048,512]{2,1,0:T(8,128)(2,1)S(1)} %copy-done, f32[1024,512]{1,0:T(8,128)} %fusion.5, bf16[1024,2048]{0,1:T(8,128)(2,1)} %bitcast.16, bf16[2048,512]{1,0:T(8,128)(2,1)} %bitcast.4), kind=kOutput, calls=%fused_computation | convolution fusion | flops 4304404480 | bytes 14684160 | tf_op jit(solution)/shard_map/dot_general | solution.py:42
  207.1 0.0 reduce-scatter.3.cloned.1.call-update
  207.1 0.0 reduce-scatter.5.cloned.1.call-start
  207.2 51.4 %reduce-scatter.3.cloned.1.call-done = bf16[1024,512]{1,0:T(8,128)(2,1)} async-done(((bf16[1024,2048]{1,0:T(8,128)(2,1)}), bf16[1024,512]{1,0:T(8,128)(2,1)}) %reduce-scatter.3.cloned.1.call-update) | async-done | bytes 1048592 | tf_op jit(solution)/shard_map/reduce_scatter | solution.py:46
  258.5 0.0 reduce-scatter.5.cloned.1.call-update
  258.6 35.4 %reduce-scatter.5.cloned.1.call-done = bf16[128,512]{1,0:T(8,128)(2,1)} async-done(((bf16[1024,512]{1,0:T(8,128)(2,1)}), bf16[128,512]{1,0:T(8,128)(2,1)}) %reduce-scatter.5.cloned.1.call-update) | async-done | bytes 131088 | tf_op jit(solution)/shard_map/reduce_scatter | solution.py:47
  294.0 3.0 copy.18
  297.0 3.0 copy.19
  (8 shorter events, 0.0 us)
Async XLA Ops:
  7.2 189.6 %copy-start = (bf16[1,2048,512]{2,1,0:T(8,128)(2,1)S(1)}, bf16[1,2048,512]{2,1,0:T(8,128)(2,1)}, u32[]{:S(2)}) copy-start(bf16[1,2048,512]{2,1,0:T(8,128)(2,1)} %param.13) | copy-start | bytes 6291460
  14.9 63.9 %all-to-all-start.1 = ((bf16[8,256,512]{2,1,0:T(8,128)(2,1)}), bf16[8,256,512]{2,1,0:T(8,128)(2,1)}, u32[]{:S(2)}, u32[]{:S(2)}) async-start(bf16[8,256,512]{2,1,0:T(8,128)(2,1)} %get-tuple-element.3), calls=%async_computation.1 | async-start | bytes 4194304 | tf_op jit(solution)/shard_map/all_to_all | solution.py:29
  21.3 34.0 %all-gather.2.cloned.1.call-start = ((), (), s32[]{:S(2)}) async-start(), calls=%async_computation.5 | async-start | bytes 1179648 | tf_op jit(solution)/shard_map/all_gather | solution.py:19
  130.6 4.6 %copy-start.1 = (f32[128,4]{0,1:T(4,128)S(1)}, f32[128,4]{0,1:T(4,128)}, u32[]{:S(2)}) copy-start(f32[128,4]{0,1:T(4,128)} %param.9) | copy-start | bytes 6148
  130.6 4.6 %copy-start.2 = (s32[128,4]{0,1:T(4,128)S(1)}, s32[128,4]{0,1:T(4,128)}, u32[]{:S(2)}) copy-start(s32[128,4]{0,1:T(4,128)} %param.8) | copy-start | bytes 6148
  130.6 66.2 %all-to-all-start = ((bf16[8,256,512]{2,1,0:T(8,128)(2,1)}), bf16[8,256,512]{2,1,0:T(8,128)(2,1)}, u32[]{:S(2)}, u32[]{:S(2)}) async-start(bf16[8,256,512]{2,1,0:T(8,128)(2,1)} %get-tuple-element.4), calls=%async_computation | async-start | bytes 4194304 | tf_op jit(solution)/shard_map/all_to_all | solution.py:29
  135.1 123.5 %reduce-scatter.3.cloned.1.call-start = ((), (), s32[]{:S(2)}) async-start(), calls=%async_computation.6 | async-start | bytes 5242880 | tf_op jit(solution)/shard_map/reduce_scatter | solution.py:46
  207.1 86.9 %reduce-scatter.5.cloned.1.call-start = ((), (), s32[]{:S(2)}) async-start(), calls=%async_computation.7 | async-start | bytes 1179648 | tf_op jit(solution)/shard_map/reduce_scatter | solution.py:47
Sparse Core Ops, SparseCore 0:
  24.2 30.9 all-gather.1
  207.2 51.2 reduce-scatter.2
  261.4 32.5 reduce-scatter.4
